TPU v7x, 32 devices: a whole 2x2x4 slice. The times are simulated.
32 devices in a mesh: dp: 4 (over y, x), kv: 4 (over z), tp: 2 (over core).
Axes of the slice: x: 2, y: 2, z: 4, core: 2. Of those that a mesh axis runs over, the one named last changes fastest.
Arguments:
- tokens: bfloat16 [16, 4, 2048], P('dp', None, ('kv', 'tp')), may hold values from -6 to 6
- lengths: int32 [16], P('dp'), may hold values from 1 to 4, 24 in all
- carried: float32 [16, 16, 128, 128], P(('dp', 'kv'), 'tp'), may hold values from -4 to 4
- norm_mix: float32 [2048], replicated, may hold values from 0.1 to 1.9
- w_query: bfloat16 [2048, 16, 128], P(None, 'tp', 'kv'), may hold values from -0.125 to 0.125
- w_forget: bfloat16 [2048, 16, 128], P(None, 'tp', 'kv'), may hold values from -0.125 to 0.125
- w_input: bfloat16 [2048, 16, 128], P(None, 'tp', 'kv'), may hold values from -0.125 to 0.125
- w_gate: bfloat16 [2048, 16, 128], P(None, 'tp', 'kv'), may hold values from -0.125 to 0.125
- lower_bound: float32 [16, 128], P('tp'), may hold values from 0.3 to 0.9
- head_gain: float32 [128], replicated, may hold values from 0.1 to 1.9
- w_out: bfloat16 [16, 128, 2048], P('tp', None, 'kv'), may hold values from -0.125 to 0.125
- mixer_norm_gain: float32 [2048], replicated, may hold values from 0.1 to 1.9
- w_up: bfloat16 [2048, 8192], P(None, ('kv', 'tp')), may hold values from -0.125 to 0.125
- w_down: bfloat16 [8192, 2048], P(('kv', 'tp')), may hold values from -0.09375 to 0.09375
Outputs:
- result: bfloat16 [16, 4, 2048], P('dp', None, ('kv', 'tp'))
- new_state: float32 [16, 16, 128, 128], P(('dp', 'kv'), 'tp')
Inputs may be any that keep to these rules, and one draw needn't show every extreme that they name: `lengths`: each sequence's number of live new token slots; some sequence has exactly 4.
All inputs are finite; a program needn't handle non-finite values. No bound on the sum of `lengths` on one device may be relied on, other than what follows from the above.
Results may differ from a plain program's by a relative error of at most 0.013.
Values may be sent and summed in bfloat16 or wider, within the bound.
A program may use at most 64 MiB of HBM per device.

v0:
```python
import functools

import jax
import jax.numpy as jnp
from jax import lax
from jax.experimental import pallas as pl
from jax.experimental.pallas import tpu as pltpu
from jax.sharding import PartitionSpec as P


def norm_rows(values, gain):
    floated = values.astype(jnp.float32)
    scaled = floated * lax.rsqrt(jnp.mean(floated * floated, axis=-1, keepdims=True) + 1e-06)
    return (scaled * gain).astype(jnp.bfloat16)


def local_collectives(
    tokens,
    lengths,
    carried,
    norm_mix,
    w_query,
    w_forget,
    w_input,
    w_gate,
    lower_bound,
    head_gain,
    w_out,
    mixer_norm_gain,
    w_up,
    w_down,
):
    tp_size = lax.axis_size("tp")
    seq_group, new_rows, piece_width = tokens.shape
    seq_dev = carried.shape[0]
    gathered = lax.all_gather(tokens, ("kv", "tp"), axis=2, tiled=True)
    normed = norm_rows(gathered, norm_mix)
    model_width = gathered.shape[2]

    def project(weight):
        return jnp.einsum(
            "snd,dhk->snhk", normed, weight, preferred_element_type=jnp.float32
        ).astype(jnp.bfloat16)

    query_raw, forget_raw, value_raw, gate_raw = (
        lax.all_to_all(project(w_query), "kv", split_axis=0, concat_axis=3, tiled=True),
        lax.all_to_all(project(w_forget), "kv", split_axis=0, concat_axis=3, tiled=True),
        lax.all_to_all(project(w_input), "kv", split_axis=0, concat_axis=3, tiled=True),
        lax.all_to_all(project(w_gate), "kv", split_axis=0, concat_axis=3, tiled=True),
    )
    own_lengths = lax.dynamic_slice_in_dim(lengths, lax.axis_index("kv") * seq_dev, seq_dev)
    query_vector = jax.nn.silu(query_raw.astype(jnp.float32))
    forget = lower_bound + (1.0 - lower_bound) * jax.nn.sigmoid(forget_raw.astype(jnp.float32))
    written = 1.0 - forget
    values = value_raw.astype(jnp.float32)
    outer_state = carried
    readouts = []
    for token_position in range(new_rows):
        alive = (token_position < own_lengths)[:, None, None, None]
        updated = (
            forget[:, token_position, :, :, None] * outer_state
            + written[:, token_position, :, :, None] * values[:, token_position, :, None, :]
        )
        outer_state = jnp.where(alive, updated, outer_state)
        state_readout = jnp.einsum(
            "shk,shkv->shv",
            query_vector[:, token_position],
            outer_state,
            precision=lax.Precision.HIGHEST,
        )
        readouts.append(jnp.where(alive[..., 0], state_readout, jnp.float32(0.0)))
    state_readout = jnp.stack(readouts, axis=1)
    scaled = state_readout * lax.rsqrt(
        jnp.mean(state_readout * state_readout, axis=-1, keepdims=True) + 1e-06
    )
    mixed = (scaled * head_gain * jax.nn.silu(gate_raw.astype(jnp.float32))).astype(jnp.bfloat16)
    branch = jnp.einsum(
        "snhv,hvd->snd",
        lax.all_gather(mixed, "kv", axis=0, tiled=True),
        w_out,
        preferred_element_type=jnp.float32,
    )
    pair_width = piece_width * tp_size
    summed_total = lax.psum(branch, "tp")
    pair_cols = lax.dynamic_slice_in_dim(gathered, lax.axis_index("kv") * pair_width, pair_width, 2)
    pair_mid = (pair_cols.astype(jnp.float32) + summed_total).astype(jnp.bfloat16)
    full_pair = lax.all_gather(pair_mid, "kv", axis=2, tiled=True)
    middle = lax.dynamic_slice_in_dim(pair_mid, lax.axis_index("tp") * piece_width, piece_width, 2)
    hidden_in = norm_rows(full_pair, mixer_norm_gain).reshape(seq_group * new_rows, model_width)
    upward = jnp.dot(hidden_in, w_up, preferred_element_type=jnp.float32)
    activated = jnp.square(jax.nn.relu(upward)).astype(jnp.bfloat16)
    collected = lax.psum_scatter(
        jnp.einsum("fd,rf->dr", w_down, activated, preferred_element_type=jnp.float32),
        ("kv", "tp"),
        scatter_dimension=0,
        tiled=True,
    )
    down_part = collected.T.reshape(seq_group, new_rows, piece_width)
    alive_rows = (jnp.arange(new_rows)[None, :] < lengths[:, None])[:, :, None]
    result = jnp.where(alive_rows, middle.astype(jnp.float32) + down_part, jnp.float32(0.0)).astype(
        jnp.bfloat16
    )
    return (result, outer_state)


MESH = pl.DeviceIdType.MESH
F32 = jnp.float32
BF16 = jnp.bfloat16


def step_kernel(
    kv_size,
    tp_size,
    tokens,
    lengths,
    carried,
    norm_mix,
    w_query,
    w_forget,
    w_input,
    w_gate,
    lower_bound,
    head_gain,
    w_out,
    mixer_gain,
    w_up,
    w_down,
    result,
    new_state,
    tok_own,
    tok_all,
    wide,
    state_v,
    state_new,
    norm_v,
    w_proj,
    w_turned,
    lower_v,
    head_v,
    w_out_v,
    mixer_v,
    w_up_v,
    w_down_v,
    raw_split,
    swap_src,
    swap_dst,
    by_slot,
    mix_src,
    mix_dst,
    mix_wide,
    pair_src,
    pair_dst,
    mid_src,
    mid_dst,
    red_src,
    red_dst,
    result_v,
    load_sem,
    send_tok,
    recv_tok,
    send_swap,
    recv_swap,
    send_mix,
    recv_mix,
    send_pair,
    recv_pair,
    send_mid,
    recv_mid,
    send_red,
    recv_red,
    store_sem,
):
    seqs, slots, piece = tok_own.shape
    group = kv_size * tp_size
    rows = seqs * slots
    heads, chans = lower_v.shape
    width = group * piece
    pair = tp_size * piece
    own_cols = w_proj.shape[1]
    sub = own_cols // heads
    per_tile = chans // sub
    kv = lax.axis_index("kv")
    tp = lax.axis_index("tp")
    me = kv * tp_size + tp

    loads = [
        pltpu.make_async_copy(tokens, tok_own, load_sem.at[0]),
        pltpu.make_async_copy(norm_mix, norm_v, load_sem.at[1]),
        pltpu.make_async_copy(w_query, w_proj.at[0], load_sem.at[2]),
        pltpu.make_async_copy(w_forget, w_proj.at[1], load_sem.at[3]),
        pltpu.make_async_copy(w_input, w_proj.at[2], load_sem.at[4]),
        pltpu.make_async_copy(w_gate, w_proj.at[3], load_sem.at[5]),
        pltpu.make_async_copy(lower_bound, lower_v, load_sem.at[6]),
        pltpu.make_async_copy(head_gain, head_v, load_sem.at[7]),
        pltpu.make_async_copy(carried, state_v, load_sem.at[8]),
        pltpu.make_async_copy(w_out, w_out_v, load_sem.at[9]),
        pltpu.make_async_copy(mixer_gain, mixer_v, load_sem.at[10]),
        pltpu.make_async_copy(w_up, w_up_v, load_sem.at[11]),
        pltpu.make_async_copy(w_down, w_down_v, load_sem.at[12]),
    ]
    early = (0, 2, 3, 4, 5, 1, 6, 7)
    for index in early:
        loads[index].start()

    mirrored = [kv, kv + 1 - 2 * lax.rem(kv, 2), lax.rem(kv + 2, 4), 3 - kv]

    def along(step):
        return mirrored[step] if kv_size == 4 else lax.rem(kv + step, kv_size)

    def peer(step):
        hop, side = divmod(step, tp_size)
        column, core = along(hop), lax.rem(tp + side, tp_size)
        return column * tp_size + core, {"kv": column, "tp": core}

    def column_peer(step):
        other = along(step)
        return other, {"kv": other, "tp": tp}

    barrier = pltpu.get_barrier_semaphore()
    for step in range(1, group):
        pl.semaphore_signal(barrier, inc=1, device_id=peer(step)[1], device_id_type=MESH)
    pl.semaphore_wait(barrier, group - 1)

    sent = []

    def send(src, dst, send_sem, recv_sem, device):
        copy = pltpu.make_async_remote_copy(
            src_ref=src,
            dst_ref=dst,
            send_sem=send_sem,
            recv_sem=recv_sem,
            device_id=device,
            device_id_type=MESH,
        )
        copy.start()
        sent.append(copy)

    def arrived(src, dst, send_sem, recv_sem, device):
        pltpu.make_async_remote_copy(
            src_ref=src,
            dst_ref=dst,
            send_sem=send_sem,
            recv_sem=recv_sem,
            device_id=device,
            device_id_type=MESH,
        ).wait_recv()

    def far_first(count):
        return range(count - 1, 0, -1)

    loads[0].wait()
    for step in far_first(group):
        _, device = peer(step)
        send(tok_own, tok_all.at[me], send_tok.at[step], recv_tok.at[me], device)
    tok_all[pl.ds(me, 1)] = tok_own[...][None]
    for index in (1, 6, 7):
        loads[index].wait()
    for matrix in range(4):
        loads[2 + matrix].wait()
        loads[8 + matrix].start()
        w_turned[matrix] = w_proj[matrix].T
    loads[12].start()
    loads[8].wait()
    state_half = state_v[...].reshape(heads * chans, chans).astype(BF16)
    for step in range(1, group):
        other, device = peer(step)
        arrived(tok_own, tok_all.at[other], send_tok.at[step], recv_tok.at[other], device)
    for part in range(group):
        block = tok_all[part].astype(F32)
        for seq in range(seqs):
            wide[seq * slots : (seq + 1) * slots, part * piece : (part + 1) * piece] = block[seq]
    floated = wide[...]
    normed = (
        floated
        * lax.rsqrt(jnp.mean(floated * floated, axis=-1, keepdims=True) + 1e-06)
        * norm_v[...]
    ).astype(BF16)
    for matrix in range(4):
        raw = jnp.dot(normed, w_turned[matrix], preferred_element_type=F32)
        for seq in range(seqs):
            raw_split[seq, matrix * slots : (matrix + 1) * slots, :] = raw[
                seq * slots : (seq + 1) * slots
            ]
    swap_src[...] = raw_split[...].astype(BF16)
    for step in far_first(kv_size):
        other, device = column_peer(step)
        send(swap_src.at[other], swap_dst.at[kv], send_swap.at[step], recv_swap.at[kv], device)
    swap_dst[pl.ds(kv, 1)] = swap_src[pl.ds(kv, 1)]
    for step in range(1, kv_size):
        other, device = column_peer(step)
        arrived(
            swap_src.at[other],
            swap_dst.at[other],
            send_swap.at[step],
            recv_swap.at[other],
            device,
        )

    lane = lax.broadcasted_iota(jnp.int32, (4 * slots, chans), 1) // sub
    arrivals = [swap_dst[part].astype(F32) for part in range(kv_size)]
    for head in range(heads):
        tile, place = divmod(head, per_tile)
        joined = None
        for part in range(kv_size):
            piece_of = arrivals[part][:, tile * chans : (tile + 1) * chans]
            shift = ((part - place) * sub) % chans
            turned = pltpu.roll(piece_of, shift, 1) if shift else piece_of
            joined = turned if joined is None else jnp.where(lane == part, turned, joined)
        by_slot[:, head, :] = joined

    length = lengths[kv]
    lower = lower_v[...]
    queries, forgets, writes, values, gates = [], [], [], [], []
    for slot in range(slots):
        alive = slot < length
        query_raw = by_slot[slot]
        gate_raw = by_slot[3 * slots + slot]
        queries.append(query_raw * jax.nn.sigmoid(query_raw))
        gates.append(gate_raw * jax.nn.sigmoid(gate_raw))
        forget = lower + (1.0 - lower) * jax.nn.sigmoid(by_slot[slots + slot])
        forgets.append(jnp.where(alive, forget, 1.0))
        writes.append(jnp.where(alive, 1.0 - forget, 0.0))
        values.append(by_slot[2 * slots + slot])
    decayed, total = [], None
    for slot in range(slots):
        total = forgets[slot] if total is None else total * forgets[slot]
        decayed.append(queries[slot] * total)
    stacked = jnp.concatenate(decayed, axis=0)
    row_head = lax.broadcasted_iota(jnp.int32, (slots * heads, chans), 0) % heads
    spread = jnp.concatenate(
        [jnp.where(row_head == head, stacked, 0.0).astype(BF16) for head in range(heads)], axis=1
    )
    from_state = jnp.dot(spread, state_half, preferred_element_type=F32)
    kept = list(writes)
    for slot in range(slots):
        for earlier in range(slot):
            kept[earlier] = kept[earlier] * forgets[slot]
        readout = from_state[slot * heads : (slot + 1) * heads]
        for earlier in range(slot + 1):
            weight = jnp.sum(queries[slot] * kept[earlier], axis=-1, keepdims=True)
            readout = readout + weight * values[earlier]
        readout = jnp.where(slot < length, readout, 0.0)
        scaled = readout * lax.rsqrt(jnp.mean(readout * readout, axis=-1, keepdims=True) + 1e-06)
        mix_src[slot] = (scaled * head_v[...] * gates[slot]).astype(BF16)
    for step in far_first(kv_size):
        other, device = column_peer(step)
        send(mix_src, mix_dst.at[kv], send_mix.at[step], recv_mix.at[kv], device)
    mix_dst[pl.ds(kv, 1)] = mix_src[...][None]

    columns = jnp.concatenate([total] + kept, axis=0).T
    for head in range(heads):
        fresh = columns[:, head : head + 1] * state_v[head]
        for slot in range(slots):
            at = (slot + 1) * heads + head
            fresh = fresh + columns[:, at : at + 1] * values[slot][head : head + 1]
        state_new[head] = fresh
    state_store = pltpu.make_async_copy(state_new, new_state, store_sem.at[0])
    state_store.start()

    for step in range(1, kv_size):
        other, device = column_peer(step)
        arrived(mix_src, mix_dst.at[other], send_mix.at[step], recv_mix.at[other], device)
    mix_wide[...] = mix_dst[...].astype(F32).reshape(rows, heads, chans)
    mixed = jnp.concatenate([mix_wide[:, head, :].astype(BF16) for head in range(heads)], axis=1)
    loads[9].wait()
    partial = jnp.dot(mixed, w_out_v[...], preferred_element_type=F32)
    pair_src[...] = partial
    partner = {"kv": kv, "tp": lax.rem(tp + 1, tp_size)}
    send(pair_src, pair_dst, send_pair.at[0], recv_pair.at[0], partner)
    own_wide = wide[:, pl.ds(pl.multiple_of(kv * pair, pair), pair)]
    arrived(pair_src, pair_dst, send_pair.at[0], recv_pair.at[0], partner)
    mid_src[...] = (own_wide + (partial + pair_dst[...])).astype(BF16)
    for step in far_first(kv_size):
        other, device = column_peer(step)
        send(mid_src, mid_dst.at[kv], send_mid.at[step], recv_mid.at[kv], device)
    mid_dst[pl.ds(kv, 1)] = mid_src[...][None]
    for step in range(1, kv_size):
        other, device = column_peer(step)
        arrived(mid_src, mid_dst.at[other], send_mid.at[step], recv_mid.at[other], device)

    middle = jnp.concatenate([mid_dst[part].astype(F32) for part in range(kv_size)], axis=1)
    loads[10].wait()
    hidden = (
        middle
        * lax.rsqrt(jnp.mean(middle * middle, axis=-1, keepdims=True) + 1e-06)
        * mixer_v[...]
    ).astype(BF16)
    loads[11].wait()
    upward = jnp.dot(hidden, w_up_v[...], preferred_element_type=F32)
    activated = jnp.square(jnp.maximum(upward, 0.0)).astype(BF16)
    loads[12].wait()

    def down_piece(other):
        cols = pl.ds(pl.multiple_of(other * piece, piece), piece)
        return jnp.dot(activated, w_down_v[:, cols], preferred_element_type=F32)

    for step in far_first(group):
        other, device = peer(step)
        red_src[step] = down_piece(other).astype(BF16)
        send(red_src.at[step], red_dst.at[me], send_red.at[step], recv_red.at[me], device)
    down = down_piece(me)
    own_mid = mid_src[:, pl.ds(pl.multiple_of(tp * piece, piece), piece)].astype(F32)
    for step in range(1, group):
        other, device = peer(step)
        arrived(red_src.at[step], red_dst.at[other], send_red.at[step], recv_red.at[other], device)
        down = down + red_dst[other].astype(F32)
    done = own_mid + down
    slot_of = lax.broadcasted_iota(jnp.int32, (slots, piece), 0)
    for seq in range(seqs):
        kept_rows = jnp.where(
            slot_of < lengths[seq], done[seq * slots : (seq + 1) * slots], 0.0
        )
        result_v[seq] = kept_rows.astype(BF16)
    result_store = pltpu.make_async_copy(result_v, result, store_sem.at[1])
    result_store.start()
    for copy in sent:
        copy.wait_send()
    state_store.wait()
    result_store.wait()


def store_kernel(result, new_state, result_out, state_out, small, large, load_sem, store_sem):
    heads = large.shape[0]
    parts = 4 if heads % 4 == 0 else 1
    chunk = heads // parts
    hops = [(result, small, result_out)]
    for part in range(parts):
        own = pl.ds(part * chunk, chunk)
        hops.append((new_state.at[own], large.at[own], state_out.at[own]))
    inward = [
        pltpu.make_async_copy(src, held, load_sem.at[at])
        for at, (src, held, _) in enumerate(hops)
    ]
    outward = [
        pltpu.make_async_copy(held, dst, store_sem.at[at])
        for at, (_, held, dst) in enumerate(hops)
    ]
    for copy in inward:
        copy.start()
    for before, after in zip(inward, outward):
        before.wait()
        after.start()
    for copy in outward:
        copy.wait()


def local_kernel(
    tokens,
    lengths,
    carried,
    norm_mix,
    w_query,
    w_forget,
    w_input,
    w_gate,
    lower_bound,
    head_gain,
    w_out,
    mixer_norm_gain,
    w_up,
    w_down,
):
    kv_size = lax.axis_size("kv")
    tp_size = lax.axis_size("tp")
    group = kv_size * tp_size
    seqs, slots, piece = tokens.shape
    _, heads, chans, _ = carried.shape
    model, _, sub = w_query.shape
    rows, pair, cols = seqs * slots, piece * tp_size, heads * sub
    hidden = w_up.shape[1]

    def turned(weight):
        return weight.transpose(1, 2, 0).reshape(cols, model)

    anywhere = pl.BlockSpec(memory_space=pl.ANY)
    dma = pltpu.SemaphoreType.DMA
    vmem = pltpu.VMEM
    result, new_state = pl.pallas_call(
        functools.partial(step_kernel, kv_size, tp_size),
        out_shape=(
            jax.ShapeDtypeStruct(tokens.shape, BF16),
            jax.ShapeDtypeStruct((heads, chans, chans), F32),
        ),
        in_specs=[anywhere, pl.BlockSpec(memory_space=pltpu.SMEM)] + [anywhere] * 12,
        out_specs=(anywhere, anywhere),
        scratch_shapes=[
            vmem((seqs, slots, piece), BF16),
            vmem((group, seqs, slots, piece), BF16),
            vmem((rows, model), F32),
            vmem((heads, chans, chans), F32),
            vmem((heads, chans, chans), F32),
            vmem((1, model), F32),
            vmem((4, cols, model), BF16),
            vmem((4, model, cols), BF16),
            vmem((heads, chans), F32),
            vmem((1, chans), F32),
            vmem((heads * chans, pair), BF16),
            vmem((1, model), F32),
            vmem((model, hidden), BF16),
            vmem((hidden, model), BF16),
            vmem((seqs, 4 * slots, cols), F32),
            vmem((seqs, 4 * slots, cols), BF16),
            vmem((kv_size, 4 * slots, cols), BF16),
            vmem((4 * slots, heads, chans), F32),
            vmem((slots, heads, chans), BF16),
            vmem((kv_size, slots, heads, chans), BF16),
            vmem((rows, heads, chans), F32),
            vmem((rows, pair), F32),
            vmem((rows, pair), F32),
            vmem((rows, pair), BF16),
            vmem((kv_size, rows, pair), BF16),
            vmem((group, rows, piece), BF16),
            vmem((group, rows, piece), BF16),
            vmem((seqs, slots, piece), BF16),
            dma((13,)),
            dma((group,)),
            dma((group,)),
            dma((kv_size,)),
            dma((kv_size,)),
            dma((kv_size,)),
            dma((kv_size,)),
            dma((1,)),
            dma((1,)),
            dma((kv_size,)),
            dma((kv_size,)),
            dma((group,)),
            dma((group,)),
            dma((2,)),
        ],
        compiler_params=pltpu.CompilerParams(
            collective_id=0, has_side_effects=True, vmem_limit_bytes=60000 * 1024
        ),
    )(
        tokens,
        lengths,
        carried.reshape(heads, chans, chans),
        norm_mix.reshape(1, model),
        turned(w_query),
        turned(w_forget),
        turned(w_input),
        turned(w_gate),
        lower_bound,
        head_gain.reshape(1, chans),
        w_out.reshape(heads * chans, pair),
        mixer_norm_gain.reshape(1, model),
        w_up,
        w_down,
    )
    result, new_state = pl.pallas_call(
        store_kernel,
        out_shape=(
            jax.ShapeDtypeStruct(tokens.shape, BF16),
            jax.ShapeDtypeStruct((heads, chans, chans), F32),
        ),
        in_specs=[anywhere] * 2,
        out_specs=(anywhere, anywhere),
        scratch_shapes=[
            vmem(tokens.shape, BF16),
            vmem((heads, chans, chans), F32),
            dma((5,)),
            dma((5,)),
        ],
        compiler_params=pltpu.CompilerParams(vmem_limit_bytes=60000 * 1024),
    )(result, new_state)
    return result, new_state.reshape(carried.shape)


def local(*arrays):
    tokens, carried, weight = arrays[0], arrays[2], arrays[4]
    aligned = (
        tokens.shape[2] % 128 == 0
        and carried.shape[0] == 1
        and carried.shape[2] % 128 == 0
        and carried.shape[2] % weight.shape[2] == 0
        and (weight.shape[1] * weight.shape[2]) % carried.shape[2] == 0
        and lax.axis_size("tp") == 2
        and tokens.shape[1] % 4 == 0
    )
    return (local_kernel if aligned else local_collectives)(*arrays)


def solution(mesh):
    placed = (
        P("dp", None, ("kv", "tp")),
        P("dp"),
        P(("dp", "kv"), "tp", None, None),
        P(),
        P(None, "tp", "kv"),
        P(None, "tp", "kv"),
        P(None, "tp", "kv"),
        P(None, "tp", "kv"),
        P("tp", None),
        P(),
        P("tp", None, "kv"),
        P(),
        P(None, ("kv", "tp")),
        P(("kv", "tp"), None),
    )
    return jax.shard_map(
        local,
        mesh=mesh,
        in_specs=placed,
        out_specs=(P("dp", None, ("kv", "tp")), P(("dp", "kv"), "tp", None, None)),
        check_vma=False,
    )
```

profile of v0, /device:TPU:0, one launch (start us, length us, event | category | flops | bytes accessed | tf_op | source)
XLA Modules:
  0.0 30.4 jit_solution(17932269926676526052)
XLA Ops:
  0.6 27.9 %shard_map.149 = (bf16[4,4,256]{2,1,0:T(4,128)(2,1)}, f32[8,128,128]{2,1,0:T(8,128)}) custom-call(bf16[4,4,256]{2,1,0:T(4,128)(2,1)} %tokens.1, s32[4]{0:T(128)} %lengths.1, f32[8,128,128]{2,1,0:T(8,128)} %bitcast.23, f32[1,2048]{1,0:T(1,128)} %bitcast.24, bf16[256,2048]{1,0:T(8,128)(2,1)} %bitcast.18, bf16[256,2048]{1,0:T(8,128)(2,1)} %bitcast.19, ...), custom_call_target="tpu_custom_call" | custom-call | tf_op jit(solution)/shard_map/pallas_call | solution.py:478
  28.6 1.9 %shard_map.150 = (bf16[4,4,256]{2,1,0:T(4,128)(2,1)}, f32[8,128,128]{2,1,0:T(8,128)}) custom-call(bf16[4,4,256]{2,1,0:T(4,128)(2,1)} %get-tuple-element.6.result, f32[8,128,128]{2,1,0:T(8,128)} %get-tuple-element.7.new_state), custom_call_target="tpu_custom_call" | custom-call | tf_op jit(solution)/shard_map/pallas_call | solution.py:549
where the time goes:
time: 30.7 us; the launch traced here: 30.4 us
  Pallas kernels  29.8 us (97%)
  between operations  0.64 us (2%)
    pallas_call x1, Pallas kernels, local_kernel(): pl.pallas_call(functools.partial(step_kernel, kv_size, tp_size), out_shap...  27.9 us
    pallas_call x1, Pallas kernels, local_kernel(): pl.pallas_call(store_kernel, out_shape=(jax.ShapeDtypeStruct(tokens.shape...  1.85 us

commit v1 on v0

v1 whole, which is shorter than its diff:
```python
import functools

import jax
import jax.numpy as jnp
from jax import lax
from jax.experimental import pallas as pl
from jax.experimental.pallas import tpu as pltpu
from jax.sharding import PartitionSpec as P


def norm_rows(values, gain):
    floated = values.astype(jnp.float32)
    scaled = floated * lax.rsqrt(jnp.mean(floated * floated, axis=-1, keepdims=True) + 1e-06)
    return (scaled * gain).astype(jnp.bfloat16)


def local_collectives(
    tokens,
    lengths,
    carried,
    norm_mix,
    w_query,
    w_forget,
    w_input,
    w_gate,
    lower_bound,
    head_gain,
    w_out,
    mixer_norm_gain,
    w_up,
    w_down,
):
    tp_size = lax.axis_size("tp")
    seq_group, new_rows, piece_width = tokens.shape
    seq_dev = carried.shape[0]
    gathered = lax.all_gather(tokens, ("kv", "tp"), axis=2, tiled=True)
    normed = norm_rows(gathered, norm_mix)
    model_width = gathered.shape[2]

    def project(weight):
        return jnp.einsum(
            "snd,dhk->snhk", normed, weight, preferred_element_type=jnp.float32
        ).astype(jnp.bfloat16)

    query_raw, forget_raw, value_raw, gate_raw = (
        lax.all_to_all(project(w_query), "kv", split_axis=0, concat_axis=3, tiled=True),
        lax.all_to_all(project(w_forget), "kv", split_axis=0, concat_axis=3, tiled=True),
        lax.all_to_all(project(w_input), "kv", split_axis=0, concat_axis=3, tiled=True),
        lax.all_to_all(project(w_gate), "kv", split_axis=0, concat_axis=3, tiled=True),
    )
    own_lengths = lax.dynamic_slice_in_dim(lengths, lax.axis_index("kv") * seq_dev, seq_dev)
    query_vector = jax.nn.silu(query_raw.astype(jnp.float32))
    forget = lower_bound + (1.0 - lower_bound) * jax.nn.sigmoid(forget_raw.astype(jnp.float32))
    written = 1.0 - forget
    values = value_raw.astype(jnp.float32)
    outer_state = carried
    readouts = []
    for token_position in range(new_rows):
        alive = (token_position < own_lengths)[:, None, None, None]
        updated = (
            forget[:, token_position, :, :, None] * outer_state
            + written[:, token_position, :, :, None] * values[:, token_position, :, None, :]
        )
        outer_state = jnp.where(alive, updated, outer_state)
        state_readout = jnp.einsum(
            "shk,shkv->shv",
            query_vector[:, token_position],
            outer_state,
            precision=lax.Precision.HIGHEST,
        )
        readouts.append(jnp.where(alive[..., 0], state_readout, jnp.float32(0.0)))
    state_readout = jnp.stack(readouts, axis=1)
    scaled = state_readout * lax.rsqrt(
        jnp.mean(state_readout * state_readout, axis=-1, keepdims=True) + 1e-06
    )
    mixed = (scaled * head_gain * jax.nn.silu(gate_raw.astype(jnp.float32))).astype(jnp.bfloat16)
    branch = jnp.einsum(
        "snhv,hvd->snd",
        lax.all_gather(mixed, "kv", axis=0, tiled=True),
        w_out,
        preferred_element_type=jnp.float32,
    )
    pair_width = piece_width * tp_size
    summed_total = lax.psum(branch, "tp")
    pair_cols = lax.dynamic_slice_in_dim(gathered, lax.axis_index("kv") * pair_width, pair_width, 2)
    pair_mid = (pair_cols.astype(jnp.float32) + summed_total).astype(jnp.bfloat16)
    full_pair = lax.all_gather(pair_mid, "kv", axis=2, tiled=True)
    middle = lax.dynamic_slice_in_dim(pair_mid, lax.axis_index("tp") * piece_width, piece_width, 2)
    hidden_in = norm_rows(full_pair, mixer_norm_gain).reshape(seq_group * new_rows, model_width)
    upward = jnp.dot(hidden_in, w_up, preferred_element_type=jnp.float32)
    activated = jnp.square(jax.nn.relu(upward)).astype(jnp.bfloat16)
    collected = lax.psum_scatter(
        jnp.einsum("fd,rf->dr", w_down, activated, preferred_element_type=jnp.float32),
        ("kv", "tp"),
        scatter_dimension=0,
        tiled=True,
    )
    down_part = collected.T.reshape(seq_group, new_rows, piece_width)
    alive_rows = (jnp.arange(new_rows)[None, :] < lengths[:, None])[:, :, None]
    result = jnp.where(alive_rows, middle.astype(jnp.float32) + down_part, jnp.float32(0.0)).astype(
        jnp.bfloat16
    )
    return (result, outer_state)


MESH = pl.DeviceIdType.MESH
F32 = jnp.float32
BF16 = jnp.bfloat16


def step_kernel(
    kv_size,
    tp_size,
    tokens,
    lengths,
    carried,
    norm_mix,
    w_query,
    w_forget,
    w_input,
    w_gate,
    lower_bound,
    head_gain,
    w_out,
    mixer_gain,
    w_up,
    w_down,
    result,
    new_state,
    tok_own,
    tok_all,
    lengths_s,
    state_v,
    norm_v,
    w_proj,
    w_turned,
    lower_v,
    head_v,
    w_out_v,
    mixer_v,
    w_up_v,
    w_down_v,
    raw_split,
    swap_src,
    swap_dst,
    by_slot,
    mix_rows,
    mix_src,
    mix_dst,
    mix_wide,
    mid_src,
    mid_dst,
    red_src,
    red_dst,
    load_sem,
    send_tok,
    recv_tok,
    send_out,
    recv_out,
    send_swap,
    recv_swap,
    send_mix,
    recv_mix,
    send_mid,
    recv_mid,
    send_red,
    recv_red,
):
    seqs, slots, piece = tok_own.shape
    group = kv_size * tp_size
    rows = seqs * slots
    heads, chans = lower_v.shape
    width = group * piece
    own_cols = w_proj.shape[1]
    sub = own_cols // heads
    per_tile = chans // sub
    kv = lax.axis_index("kv")
    tp = lax.axis_index("tp")
    me = kv * tp_size + tp
    mate = tp_size - 1 - tp

    mirrored = [kv, kv + 1 - 2 * lax.rem(kv, 2), lax.rem(kv + 2, 4), 3 - kv]

    def along(step):
        return mirrored[step] if kv_size == 4 else lax.rem(kv + step, kv_size)

    def place(column, core):
        return column * tp_size + core, {"kv": column, "tp": core}

    far_peers = [
        place(along(hop), core) for hop in range(kv_size - 1, 0, -1) for core in range(tp_size)
    ]
    far_peers.append(place(kv, mate))
    near_peers = [place(kv, mate)] + [
        place(along(hop), core)
        for hop in range(1, kv_size)
        for core in range(tp_size - 1, -1, -1)
    ]
    far_columns = [place(along(hop), tp) for hop in range(kv_size - 1, 0, -1)]
    near_columns = far_columns[::-1]

    barrier = pltpu.get_barrier_semaphore()
    for _, device in far_peers:
        pl.semaphore_signal(barrier, inc=1, device_id=device, device_id_type=MESH)

    own_out = pl.ds(pl.multiple_of(tp * piece, piece), piece)
    mate_out = pl.ds(pl.multiple_of(mate * piece, piece), piece)
    loads = [
        pltpu.make_async_copy(tokens, tok_own, load_sem.at[0]),
        pltpu.make_async_copy(norm_mix, norm_v, load_sem.at[1]),
        pltpu.make_async_copy(w_query, w_proj.at[0], load_sem.at[2]),
        pltpu.make_async_copy(w_forget, w_proj.at[1], load_sem.at[3]),
        pltpu.make_async_copy(w_input, w_proj.at[2], load_sem.at[4]),
        pltpu.make_async_copy(w_gate, w_proj.at[3], load_sem.at[5]),
        pltpu.make_async_copy(lower_bound, lower_v, load_sem.at[6]),
        pltpu.make_async_copy(head_gain, head_v, load_sem.at[7]),
        pltpu.make_async_copy(carried, state_v, load_sem.at[8]),
        pltpu.make_async_copy(w_out.at[:, own_out], w_out_v.at[tp], load_sem.at[9]),
        pltpu.make_async_copy(mixer_gain, mixer_v, load_sem.at[10]),
        pltpu.make_async_copy(w_up, w_up_v, load_sem.at[11]),
        pltpu.make_async_copy(w_down, w_down_v, load_sem.at[12]),
        pltpu.make_async_copy(lengths, lengths_s, load_sem.at[13]),
    ]
    for index in (0, 2, 3, 4, 5, 1, 6, 7, 13):
        loads[index].start()

    sent = []

    def remote(src, dst, send_sem, recv_sem, device):
        return pltpu.make_async_remote_copy(
            src_ref=src,
            dst_ref=dst,
            send_sem=send_sem,
            recv_sem=recv_sem,
            device_id=device,
            device_id_type=MESH,
        )

    def send(*parts):
        copy = remote(*parts)
        copy.start()
        sent.append(copy)

    def arrived(*parts):
        remote(*parts).wait_recv()

    pl.semaphore_wait(barrier, group - 1)
    loads[0].wait()
    for other, device in far_peers:
        send(tok_own, tok_all.at[me], send_tok.at[other], recv_tok.at[me], device)
    mate_device = place(kv, mate)[1]
    send(w_out.at[:, mate_out], w_out_v.at[tp], send_out.at[0], recv_out.at[0], mate_device)
    for matrix in range(4):
        loads[2 + matrix].wait()
        loads[8 + matrix].start()
        w_turned[:, matrix * own_cols : (matrix + 1) * own_cols] = w_proj[matrix].T
    loads[12].start()
    loads[8].wait()
    state_half = state_v[...].reshape(heads * chans, chans).astype(BF16)
    for index in (1, 6, 7, 13):
        loads[index].wait()

    def stack_rows(block):
        return jnp.concatenate([block[seq].astype(F32) for seq in range(seqs)], axis=0)

    def folded(values):
        total = None
        for at in range(0, piece, chans):
            part = values[:, at : at + chans]
            total = part * part if total is None else total + part * part
        return total

    def span(part):
        return pl.ds(pl.multiple_of(part * piece, piece), piece)

    own_tok = stack_rows(tok_own[...])
    squares = folded(own_tok)
    raw = jnp.dot(
        (own_tok * norm_v[:, span(me)]).astype(BF16),
        w_turned[span(me), :],
        preferred_element_type=F32,
    )
    for other, device in near_peers:
        arrived(tok_own, tok_all.at[other], send_tok.at[other], recv_tok.at[other], device)
        block = stack_rows(tok_all[other])
        squares = squares + folded(block)
        raw = raw + jnp.dot(
            (block * norm_v[:, span(other)]).astype(BF16),
            w_turned[span(other), :],
            preferred_element_type=F32,
        )
    raw = raw * lax.rsqrt(jnp.sum(squares, axis=-1, keepdims=True) / width + 1e-06)
    for matrix in range(4):
        for seq in range(seqs):
            raw_split[seq, matrix * slots : (matrix + 1) * slots, :] = raw[
                seq * slots : (seq + 1) * slots, matrix * own_cols : (matrix + 1) * own_cols
            ]
    swap_src[...] = raw_split[...].astype(BF16)
    for other, device in far_columns:
        column = device["kv"]
        send(swap_src.at[column], swap_dst.at[kv], send_swap.at[column], recv_swap.at[kv], device)
    swap_dst[pl.ds(kv, 1)] = swap_src[pl.ds(kv, 1)]
    for other, device in near_columns:
        column = device["kv"]
        arrived(
            swap_src.at[column],
            swap_dst.at[column],
            send_swap.at[column],
            recv_swap.at[column],
            device,
        )

    lane = lax.broadcasted_iota(jnp.int32, (4 * slots, chans), 1) // sub
    arrivals = [swap_dst[part].astype(F32) for part in range(kv_size)]
    for head in range(heads):
        tile, spot = divmod(head, per_tile)
        joined = None
        for part in range(kv_size):
            piece_of = arrivals[part][:, tile * chans : (tile + 1) * chans]
            shift = ((part - spot) * sub) % chans
            turned = pltpu.roll(piece_of, shift, 1) if shift else piece_of
            joined = turned if joined is None else jnp.where(lane == part, turned, joined)
        by_slot[:, head, :] = joined

    length = lengths_s[kv]
    lower = lower_v[...]
    queries, forgets, writes, values, gates = [], [], [], [], []
    for slot in range(slots):
        alive = slot < length
        query_raw = by_slot[slot]
        gate_raw = by_slot[3 * slots + slot]
        queries.append(query_raw * jax.nn.sigmoid(query_raw))
        gates.append(gate_raw * jax.nn.sigmoid(gate_raw))
        forget = lower + (1.0 - lower) * jax.nn.sigmoid(by_slot[slots + slot])
        forgets.append(jnp.where(alive, forget, 1.0))
        writes.append(jnp.where(alive, 1.0 - forget, 0.0))
        values.append(by_slot[2 * slots + slot])
    decayed, total = [], None
    for slot in range(slots):
        total = forgets[slot] if total is None else total * forgets[slot]
        decayed.append(queries[slot] * total)
    stacked = jnp.concatenate(decayed, axis=0)
    row_head = lax.broadcasted_iota(jnp.int32, (slots * heads, chans), 0) % heads
    spread = jnp.concatenate(
        [jnp.where(row_head == head, stacked, 0.0).astype(BF16) for head in range(heads)], axis=1
    )
    from_state = jnp.dot(spread, state_half, preferred_element_type=F32)
    kept = list(writes)
    for slot in range(slots):
        for earlier in range(slot):
            kept[earlier] = kept[earlier] * forgets[slot]
        readout = from_state[slot * heads : (slot + 1) * heads]
        for earlier in range(slot + 1):
            weight = jnp.sum(queries[slot] * kept[earlier], axis=-1, keepdims=True)
            readout = readout + weight * values[earlier]
        readout = jnp.where(slot < length, readout, 0.0)
        scaled = readout * lax.rsqrt(jnp.mean(readout * readout, axis=-1, keepdims=True) + 1e-06)
        mix_rows[slot] = scaled * head_v[...] * gates[slot]
    for head in range(heads):
        mix_src[:, head * chans : (head + 1) * chans] = mix_rows[:, head, :].astype(BF16)
    for other, device in far_peers:
        send(mix_src, mix_dst.at[me], send_mix.at[other], recv_mix.at[me], device)

    columns = jnp.concatenate([total] + kept, axis=0).T
    for head in range(heads):
        fresh = columns[:, head : head + 1] * state_v[head]
        for slot in range(slots):
            at = (slot + 1) * heads + head
            fresh = fresh + columns[:, at : at + 1] * values[slot][head : head + 1]
        new_state[head] = fresh

    loads[9].wait()
    arrived(w_out.at[:, mate_out], w_out_v.at[mate], send_out.at[0], recv_out.at[0], mate_device)
    mix_dst[pl.ds(me, 1)] = mix_src[...][None]
    for other, device in near_peers:
        arrived(mix_src, mix_dst.at[other], send_mix.at[other], recv_mix.at[other], device)
    for column in range(kv_size):
        for core in range(tp_size):
            mix_wide[core, column * slots : (column + 1) * slots, :] = mix_dst[
                column * tp_size + core
            ].astype(F32)
    middle = own_tok
    for core in range(tp_size):
        middle = middle + jnp.dot(
            mix_wide[core].astype(BF16), w_out_v[core], preferred_element_type=F32
        )
    mid_src[...] = middle.astype(BF16)
    for other, device in far_peers:
        send(mid_src, mid_dst.at[me], send_mid.at[other], recv_mid.at[me], device)

    loads[10].wait()
    loads[11].wait()
    own_mid = mid_src[...].astype(F32)
    squares = folded(own_mid)
    upward = jnp.dot(
        (own_mid * mixer_v[:, span(me)]).astype(BF16),
        w_up_v[span(me), :],
        preferred_element_type=F32,
    )
    for other, device in near_peers:
        arrived(mid_src, mid_dst.at[other], send_mid.at[other], recv_mid.at[other], device)
        block = mid_dst[other].astype(F32)
        squares = squares + folded(block)
        upward = upward + jnp.dot(
            (block * mixer_v[:, span(other)]).astype(BF16),
            w_up_v[span(other), :],
            preferred_element_type=F32,
        )
    upward = upward * lax.rsqrt(jnp.sum(squares, axis=-1, keepdims=True) / width + 1e-06)
    activated = jnp.square(jnp.maximum(upward, 0.0)).astype(BF16)
    loads[12].wait()

    def down_piece(other):
        return jnp.dot(activated, w_down_v[:, span(other)], preferred_element_type=F32)

    for other, device in far_peers:
        red_src[other] = down_piece(other).astype(BF16)
        send(red_src.at[other], red_dst.at[me], send_red.at[other], recv_red.at[me], device)
    done = own_mid + down_piece(me)
    for other, device in near_peers:
        arrived(red_src.at[other], red_dst.at[other], send_red.at[other], recv_red.at[other], device)
        done = done + red_dst[other].astype(F32)
    slot_of = lax.broadcasted_iota(jnp.int32, (slots, piece), 0)
    for seq in range(seqs):
        kept_rows = jnp.where(
            slot_of < lengths_s[seq], done[seq * slots : (seq + 1) * slots], 0.0
        )
        result[seq] = kept_rows.astype(BF16)
    for copy in sent:
        copy.wait_send()


def store_kernel(result, new_state, result_out, state_out, store_sem):
    heads = new_state.shape[0]
    parts = 4 if heads % 4 == 0 else 1
    chunk = heads // parts
    copies = [pltpu.make_async_copy(result, result_out, store_sem.at[parts])]
    for part in range(parts):
        own = pl.ds(part * chunk, chunk)
        copies.append(
            pltpu.make_async_copy(new_state.at[own], state_out.at[own], store_sem.at[part])
        )
    for copy in copies:
        copy.start()
    for copy in copies:
        copy.wait()


def local_kernel(
    tokens,
    lengths,
    carried,
    norm_mix,
    w_query,
    w_forget,
    w_input,
    w_gate,
    lower_bound,
    head_gain,
    w_out,
    mixer_norm_gain,
    w_up,
    w_down,
):
    kv_size = lax.axis_size("kv")
    tp_size = lax.axis_size("tp")
    group = kv_size * tp_size
    seqs, slots, piece = tokens.shape
    _, heads, chans, _ = carried.shape
    model, _, sub = w_query.shape
    rows, pair, cols = seqs * slots, piece * tp_size, heads * sub
    hidden = w_up.shape[1]

    def turned(weight):
        return weight.transpose(1, 2, 0).reshape(cols, model)

    anywhere = pl.BlockSpec(memory_space=pl.ANY)
    inside = pl.BlockSpec(memory_space=pltpu.VMEM)
    outside = pl.BlockSpec(memory_space=pltpu.HBM)
    dma = pltpu.SemaphoreType.DMA
    vmem = pltpu.VMEM
    result, new_state = pl.pallas_call(
        functools.partial(step_kernel, kv_size, tp_size),
        out_shape=(
            vmem(tokens.shape, BF16),
            vmem((heads, chans, chans), F32),
        ),
        in_specs=[outside] * 14,
        out_specs=(inside, inside),
        scratch_shapes=[
            vmem((seqs, slots, piece), BF16),
            vmem((group, seqs, slots, piece), BF16),
            pltpu.SMEM((seqs,), jnp.int32),
            vmem((heads, chans, chans), F32),
            vmem((1, model), F32),
            vmem((4, cols, model), BF16),
            vmem((model, 4 * cols), BF16),
            vmem((heads, chans), F32),
            vmem((1, chans), F32),
            vmem((tp_size, heads * chans, piece), BF16),
            vmem((1, model), F32),
            vmem((model, hidden), BF16),
            vmem((hidden, model), BF16),
            vmem((seqs, 4 * slots, cols), F32),
            vmem((seqs, 4 * slots, cols), BF16),
            vmem((kv_size, 4 * slots, cols), BF16),
            vmem((4 * slots, heads, chans), F32),
            vmem((slots, heads, chans), F32),
            vmem((slots, heads * chans), BF16),
            vmem((group, slots, heads * chans), BF16),
            vmem((tp_size, rows, heads * chans), F32),
            vmem((rows, piece), BF16),
            vmem((group, rows, piece), BF16),
            vmem((group, rows, piece), BF16),
            vmem((group, rows, piece), BF16),
            dma((14,)),
            dma((group,)),
            dma((group,)),
            dma((1,)),
            dma((1,)),
            dma((kv_size,)),
            dma((kv_size,)),
            dma((group,)),
            dma((group,)),
            dma((group,)),
            dma((group,)),
            dma((group,)),
            dma((group,)),
        ],
        compiler_params=pltpu.CompilerParams(
            collective_id=0, has_side_effects=True, vmem_limit_bytes=56000 * 1024
        ),
    )(
        tokens,
        lengths,
        carried.reshape(heads, chans, chans),
        norm_mix.reshape(1, model),
        turned(w_query),
        turned(w_forget),
        turned(w_input),
        turned(w_gate),
        lower_bound,
        head_gain.reshape(1, chans),
        w_out.reshape(heads * chans, pair),
        mixer_norm_gain.reshape(1, model),
        w_up,
        w_down,
    )
    result, new_state = pl.pallas_call(
        store_kernel,
        out_shape=(
            jax.ShapeDtypeStruct(tokens.shape, BF16),
            jax.ShapeDtypeStruct((heads, chans, chans), F32),
        ),
        in_specs=[inside] * 2,
        out_specs=(anywhere, anywhere),
        scratch_shapes=[dma((5,))],
        compiler_params=pltpu.CompilerParams(vmem_limit_bytes=4000 * 1024),
    )(result, new_state)
    return result, new_state.reshape(carried.shape)


def local(*arrays):
    tokens, carried, weight = arrays[0], arrays[2], arrays[4]
    aligned = (
        tokens.shape[2] % 128 == 0
        and carried.shape[0] == 1
        and carried.shape[2] % 128 == 0
        and carried.shape[2] % weight.shape[2] == 0
        and (weight.shape[1] * weight.shape[2]) % carried.shape[2] == 0
        and lax.axis_size("tp") == 2
        and tokens.shape[1] % 4 == 0
    )
    return (local_kernel if aligned else local_collectives)(*arrays)


def solution(mesh):
    placed = (
        P("dp", None, ("kv", "tp")),
        P("dp"),
        P(("dp", "kv"), "tp", None, None),
        P(),
        P(None, "tp", "kv"),
        P(None, "tp", "kv"),
        P(None, "tp", "kv"),
        P(None, "tp", "kv"),
        P("tp", None),
        P(),
        P("tp", None, "kv"),
        P(),
        P(None, ("kv", "tp")),
        P(("kv", "tp"), None),
    )
    return jax.shard_map(
        local,
        mesh=mesh,
        in_specs=placed,
        out_specs=(P("dp", None, ("kv", "tp")), P(("dp", "kv"), "tp", None, None)),
        check_vma=False,
    )
```

time: 30.7 us -> 27.4 us (0.89)
  Pallas kernels: 29.8 us -> 26.6 us
    pallas_call x1, Pallas kernels: 27.9 us -> 25.8 us  [local_kernel(): pl.pallas_call(functools.partial(step_kernel, kv_size, tp_size), out_shap...]
    pallas_call x1, Pallas kernels: 1.85 us -> 0.83 us  [local_kernel(): pl.pallas_call(store_kernel, out_shape=(jax.ShapeDtypeStruct(tokens.shape...]
where the time goes in v1:
time: 27.4 us; the launch traced here: 27.2 us
  Pallas kernels  26.6 us (97%)
  between operations  0.64 us (2%)
    pallas_call x1, Pallas kernels, local_kernel(): pl.pallas_call(functools.partial(step_kernel, kv_size, tp_size), out_shap...  25.8 us
    pallas_call x1, Pallas kernels, local_kernel(): pl.pallas_call(store_kernel, out_shape=(jax.ShapeDtypeStruct(tokens.shape...  0.83 us

profile of v1, /device:TPU:0, one launch (start us, length us, event | category | flops | bytes accessed | tf_op | source)
XLA Modules:
  0.0 27.2 jit_solution(13853664027226187671)
XLA Ops:
  0.6 25.8 %shard_map.149 = (bf16[4,4,256]{2,1,0:T(4,128)(2,1)S(1)}, f32[8,128,128]{2,1,0:T(8,128)S(1)}) custom-call(bf16[4,4,256]{2,1,0:T(4,128)(2,1)} %tokens.1, s32[4]{0:T(128)} %lengths.1, f32[8,128,128]{2,1,0:T(8,128)} %bitcast.23, f32[1,2048]{1,0:T(1,128)} %bitcast.24, bf16[256,2048]{1,0:T(8,128)(2,1)} %bitcast.18, bf16[256,2048]{1,0:T(8,128)(2,1)} %bitcast.19, ...), custom_call_target="tpu_custom_call" | custom-call | tf_op jit(solution)/shard_map/pallas_call | solution.py:482
  26.4 0.8 %shard_map.150 = (bf16[4,4,256]{2,1,0:T(4,128)(2,1)}, f32[8,128,128]{2,1,0:T(8,128)}) custom-call(bf16[4,4,256]{2,1,0:T(4,128)(2,1)S(1)} %get-tuple-element.6.result, f32[8,128,128]{2,1,0:T(8,128)S(1)} %get-tuple-element.7.new_state), custom_call_target="tpu_custom_call" | custom-call | tf_op jit(solution)/shard_map/pallas_call | solution.py:549

commit v2 on v1

--- a/solution.py
+++ b/solution.py
@@ -141,6 +141,7 @@
     w_up_v,
     w_down_v,
     raw_split,
+    scale_v,
     swap_src,
     swap_dst,
     by_slot,
@@ -153,24 +154,18 @@
     red_src,
     red_dst,
     load_sem,
-    send_tok,
-    recv_tok,
-    send_out,
+    entered,
+    send_sem,
     recv_out,
-    send_swap,
     recv_swap,
-    send_mix,
-    recv_mix,
-    send_mid,
-    recv_mid,
-    send_red,
-    recv_red,
+    recv_wide,
+    recv_near,
 ):
     seqs, slots, piece = tok_own.shape
     group = kv_size * tp_size
-    rows = seqs * slots
     heads, chans = lower_v.shape
     width = group * piece
+    pair = tp_size * piece
     own_cols = w_proj.shape[1]
     sub = own_cols // heads
     per_tile = chans // sub
@@ -179,138 +174,169 @@
     me = kv * tp_size + tp
     mate = tp_size - 1 - tp
 
+    token_load = pltpu.make_async_copy(tokens, tok_own, load_sem.at[0])
+    token_load.start()
+
     mirrored = [kv, kv + 1 - 2 * lax.rem(kv, 2), lax.rem(kv + 2, 4), 3 - kv]
 
     def along(step):
         return mirrored[step] if kv_size == 4 else lax.rem(kv + step, kv_size)
 
-    def place(column, core):
-        return column * tp_size + core, {"kv": column, "tp": core}
-
-    far_peers = [
-        place(along(hop), core) for hop in range(kv_size - 1, 0, -1) for core in range(tp_size)
-    ]
-    far_peers.append(place(kv, mate))
-    near_peers = [place(kv, mate)] + [
-        place(along(hop), core)
-        for hop in range(1, kv_size)
-        for core in range(tp_size - 1, -1, -1)
-    ]
-    far_columns = [place(along(hop), tp) for hop in range(kv_size - 1, 0, -1)]
-    near_columns = far_columns[::-1]
+    near_columns = [along(hop) for hop in range(1, kv_size)]
+    far_columns = near_columns[::-1]
+    mate_device = {"kv": kv, "tp": mate}
+
+    def cores(column):
+        return [{"kv": column, "tp": core} for core in range(tp_size)]
 
     barrier = pltpu.get_barrier_semaphore()
-    for _, device in far_peers:
-        pl.semaphore_signal(barrier, inc=1, device_id=device, device_id_type=MESH)
+    pl.semaphore_signal(barrier, inc=1, device_id=mate_device, device_id_type=MESH)
+    for column in near_columns:
+
+        @pl.when(column > kv)
+        def _():
+            for device in cores(column):
+                pl.semaphore_signal(barrier, inc=1, device_id=device, device_id_type=MESH)
 
     own_out = pl.ds(pl.multiple_of(tp * piece, piece), piece)
     mate_out = pl.ds(pl.multiple_of(mate * piece, piece), piece)
-    loads = [
-        pltpu.make_async_copy(tokens, tok_own, load_sem.at[0]),
-        pltpu.make_async_copy(norm_mix, norm_v, load_sem.at[1]),
-        pltpu.make_async_copy(w_query, w_proj.at[0], load_sem.at[2]),
-        pltpu.make_async_copy(w_forget, w_proj.at[1], load_sem.at[3]),
-        pltpu.make_async_copy(w_input, w_proj.at[2], load_sem.at[4]),
-        pltpu.make_async_copy(w_gate, w_proj.at[3], load_sem.at[5]),
+    matrix_loads = [
+        pltpu.make_async_copy(weight, w_proj.at[at], load_sem.at[1 + at])
+        for at, weight in enumerate((w_query, w_forget, w_input, w_gate))
+    ]
+    small_loads = [
+        pltpu.make_async_copy(norm_mix, norm_v, load_sem.at[5]),
         pltpu.make_async_copy(lower_bound, lower_v, load_sem.at[6]),
         pltpu.make_async_copy(head_gain, head_v, load_sem.at[7]),
-        pltpu.make_async_copy(carried, state_v, load_sem.at[8]),
-        pltpu.make_async_copy(w_out.at[:, own_out], w_out_v.at[tp], load_sem.at[9]),
-        pltpu.make_async_copy(mixer_gain, mixer_v, load_sem.at[10]),
-        pltpu.make_async_copy(w_up, w_up_v, load_sem.at[11]),
-        pltpu.make_async_copy(w_down, w_down_v, load_sem.at[12]),
-        pltpu.make_async_copy(lengths, lengths_s, load_sem.at[13]),
+        pltpu.make_async_copy(lengths, lengths_s, load_sem.at[8]),
     ]
-    for index in (0, 2, 3, 4, 5, 1, 6, 7, 13):
-        loads[index].start()
-
-    sent = []
-
-    def remote(src, dst, send_sem, recv_sem, device):
+    state_load = pltpu.make_async_copy(carried, state_v, load_sem.at[1])
+    out_load = pltpu.make_async_copy(w_out.at[:, own_out], w_out_v.at[tp], load_sem.at[2])
+    mixer_load = pltpu.make_async_copy(mixer_gain, mixer_v, load_sem.at[3])
+    up_load = pltpu.make_async_copy(w_up, w_up_v, load_sem.at[4])
+    down_load = pltpu.make_async_copy(w_down, w_down_v, load_sem.at[0])
+    for copy in matrix_loads + small_loads:
+        copy.start()
+
+    def remote(src, dst, phase, recv_sem, device):
         return pltpu.make_async_remote_copy(
             src_ref=src,
             dst_ref=dst,
-            send_sem=send_sem,
+            send_sem=send_sem.at[phase],
             recv_sem=recv_sem,
             device_id=device,
             device_id_type=MESH,
         )
 
-    def send(*parts):
-        copy = remote(*parts)
-        copy.start()
-        sent.append(copy)
-
-    def arrived(*parts):
-        remote(*parts).wait_recv()
-
-    pl.semaphore_wait(barrier, group - 1)
-    loads[0].wait()
-    for other, device in far_peers:
-        send(tok_own, tok_all.at[me], send_tok.at[other], recv_tok.at[me], device)
-    mate_device = place(kv, mate)[1]
-    send(w_out.at[:, mate_out], w_out_v.at[tp], send_out.at[0], recv_out.at[0], mate_device)
+    def arrived(ref, recv_sem):
+        remote(ref, ref, 0, recv_sem, mate_device).wait_recv()
+
+    def duo(column):
+        return pl.ds(pl.multiple_of(column * tp_size, tp_size), tp_size)
+
+    def span(part):
+        return pl.ds(pl.multiple_of(part * pair, pair), pair)
+
+    def give_tokens(device):
+        remote(tok_own, tok_all.at[me], 0, recv_wide.at[kv], device).start()
+
+    pl.semaphore_wait(barrier, tp_size * kv + tp_size - 1)
+    for column in far_columns:
+
+        @pl.when(column < kv)
+        def _():
+            for device in cores(column):
+                pl.semaphore_signal(
+                    entered.at[kv], inc=1, device_id=device, device_id_type=MESH
+                )
+
+    token_load.wait()
+    for column in far_columns:
+
+        @pl.when(column < kv)
+        def _():
+            for device in cores(column):
+                give_tokens(device)
+
+    give_tokens(mate_device)
+    tok_all[pl.ds(me, 1)] = tok_own[...][None]
+    later = [state_load, out_load, mixer_load, up_load]
     for matrix in range(4):
-        loads[2 + matrix].wait()
-        loads[8 + matrix].start()
+        matrix_loads[matrix].wait()
+        later[matrix].start()
         w_turned[:, matrix * own_cols : (matrix + 1) * own_cols] = w_proj[matrix].T
-    loads[12].start()
-    loads[8].wait()
+    down_load.start()
+    for column in near_columns:
+
+        @pl.when(column > kv)
+        def _():
+            pl.semaphore_wait(entered.at[column], tp_size)
+            for device in cores(column):
+                give_tokens(device)
+
+    remote(w_out.at[:, mate_out], w_out_v.at[tp], 1, recv_out.at[0], mate_device).start()
+    state_load.wait()
     state_half = state_v[...].reshape(heads * chans, chans).astype(BF16)
-    for index in (1, 6, 7, 13):
-        loads[index].wait()
-
-    def stack_rows(block):
-        return jnp.concatenate([block[seq].astype(F32) for seq in range(seqs)], axis=0)
+    for copy in small_loads:
+        copy.wait()
 
     def folded(values):
         total = None
-        for at in range(0, piece, chans):
+        for at in range(0, pair, chans):
             part = values[:, at : at + chans]
             total = part * part if total is None else total + part * part
         return total
 
-    def span(part):
-        return pl.ds(pl.multiple_of(part * piece, piece), piece)
-
-    own_tok = stack_rows(tok_own[...])
-    squares = folded(own_tok)
-    raw = jnp.dot(
-        (own_tok * norm_v[:, span(me)]).astype(BF16),
-        w_turned[span(me), :],
-        preferred_element_type=F32,
-    )
-    for other, device in near_peers:
-        arrived(tok_own, tok_all.at[other], send_tok.at[other], recv_tok.at[other], device)
-        block = stack_rows(tok_all[other])
-        squares = squares + folded(block)
-        raw = raw + jnp.dot(
-            (block * norm_v[:, span(other)]).astype(BF16),
-            w_turned[span(other), :],
+    def tokens_of(column):
+        halves = []
+        for core in range(tp_size):
+            block = tok_all[column * tp_size + core]
+            halves.append(
+                jnp.concatenate([block[seq].astype(F32) for seq in range(seqs)], axis=0)
+            )
+        return jnp.concatenate(halves, axis=1)
+
+    def gained(block, gain, weights, column):
+        return jnp.dot(
+            (block * gain[:, span(column)]).astype(BF16),
+            weights[span(column), :],
             preferred_element_type=F32,
         )
-    raw = raw * lax.rsqrt(jnp.sum(squares, axis=-1, keepdims=True) / width + 1e-06)
+
+    raw, squares = None, None
+    for column in [kv] + near_columns:
+        if raw is None:
+            arrived(tok_all.at[kv * tp_size + mate], recv_wide.at[kv])
+        else:
+            arrived(tok_all.at[duo(column)], recv_wide.at[column])
+        block = tokens_of(column)
+        product = gained(block, norm_v, w_turned, column)
+        raw = product if raw is None else raw + product
+        squares = folded(block) if squares is None else squares + folded(block)
     for matrix in range(4):
         for seq in range(seqs):
             raw_split[seq, matrix * slots : (matrix + 1) * slots, :] = raw[
                 seq * slots : (seq + 1) * slots, matrix * own_cols : (matrix + 1) * own_cols
             ]
     swap_src[...] = raw_split[...].astype(BF16)
-    for other, device in far_columns:
-        column = device["kv"]
-        send(swap_src.at[column], swap_dst.at[kv], send_swap.at[column], recv_swap.at[kv], device)
+    for column in far_columns:
+        remote(
+            swap_src.at[column],
+            swap_dst.at[kv],
+            2,
+            recv_swap.at[0],
+            {"kv": column, "tp": tp},
+        ).start()
     swap_dst[pl.ds(kv, 1)] = swap_src[pl.ds(kv, 1)]
-    for other, device in near_columns:
-        column = device["kv"]
-        arrived(
-            swap_src.at[column],
-            swap_dst.at[column],
-            send_swap.at[column],
-            recv_swap.at[column],
-            device,
-        )
-
+    factor = lax.rsqrt(jnp.sum(squares, axis=-1, keepdims=True) / width + 1e-06)
+    for seq in range(seqs):
+        scale_v[seq] = jnp.broadcast_to(factor[seq * slots : (seq + 1) * slots], (slots, chans))
+    own_scale = scale_v[kv]
+    length = lengths_s[kv]
+    lower = lower_v[...]
     lane = lax.broadcasted_iota(jnp.int32, (4 * slots, chans), 1) // sub
+    arrived(swap_dst.at[pl.ds(0, kv_size - 1)], recv_swap.at[0])
+
     arrivals = [swap_dst[part].astype(F32) for part in range(kv_size)]
     for head in range(heads):
         tile, spot = divmod(head, per_tile)
@@ -322,19 +348,18 @@
             joined = turned if joined is None else jnp.where(lane == part, turned, joined)
         by_slot[:, head, :] = joined
 
-    length = lengths_s[kv]
-    lower = lower_v[...]
     queries, forgets, writes, values, gates = [], [], [], [], []
     for slot in range(slots):
         alive = slot < length
-        query_raw = by_slot[slot]
-        gate_raw = by_slot[3 * slots + slot]
+        scale = own_scale[slot : slot + 1]
+        query_raw = by_slot[slot] * scale
+        gate_raw = by_slot[3 * slots + slot] * scale
         queries.append(query_raw * jax.nn.sigmoid(query_raw))
         gates.append(gate_raw * jax.nn.sigmoid(gate_raw))
-        forget = lower + (1.0 - lower) * jax.nn.sigmoid(by_slot[slots + slot])
+        forget = lower + (1.0 - lower) * jax.nn.sigmoid(by_slot[slots + slot] * scale)
         forgets.append(jnp.where(alive, forget, 1.0))
         writes.append(jnp.where(alive, 1.0 - forget, 0.0))
-        values.append(by_slot[2 * slots + slot])
+        values.append(by_slot[2 * slots + slot] * scale)
     decayed, total = [], None
     for slot in range(slots):
         total = forgets[slot] if total is None else total * forgets[slot]
@@ -358,8 +383,10 @@
         mix_rows[slot] = scaled * head_v[...] * gates[slot]
     for head in range(heads):
         mix_src[:, head * chans : (head + 1) * chans] = mix_rows[:, head, :].astype(BF16)
-    for other, device in far_peers:
-        send(mix_src, mix_dst.at[me], send_mix.at[other], recv_mix.at[me], device)
+    for column in far_columns:
+        for device in cores(column):
+            remote(mix_src, mix_dst.at[me], 3, recv_near.at[kv], device).start()
+    remote(mix_src, mix_dst.at[me], 3, recv_near.at[kv], mate_device).start()
 
     columns = jnp.concatenate([total] + kept, axis=0).T
     for head in range(heads):
@@ -369,65 +396,90 @@
             fresh = fresh + columns[:, at : at + 1] * values[slot][head : head + 1]
         new_state[head] = fresh
 
-    loads[9].wait()
-    arrived(w_out.at[:, mate_out], w_out_v.at[mate], send_out.at[0], recv_out.at[0], mate_device)
+    out_load.wait()
+    mixer_load.wait()
+    up_load.wait()
+    down_load.wait()
+    arrived(w_out_v.at[mate], recv_out.at[0])
     mix_dst[pl.ds(me, 1)] = mix_src[...][None]
-    for other, device in near_peers:
-        arrived(mix_src, mix_dst.at[other], send_mix.at[other], recv_mix.at[other], device)
-    for column in range(kv_size):
+    for column in [kv] + near_columns:
+        if column is kv:
+            arrived(mix_dst.at[kv * tp_size + mate], recv_near.at[kv])
+        else:
+            arrived(mix_dst.at[duo(column)], recv_near.at[column])
         for core in range(tp_size):
-            mix_wide[core, column * slots : (column + 1) * slots, :] = mix_dst[
-                column * tp_size + core
-            ].astype(F32)
-    middle = own_tok
+            mix_wide[core, column] = mix_dst[column * tp_size + core].astype(F32)
+    middle = jnp.concatenate([tok_own[seq].astype(F32) for seq in range(seqs)], axis=0)
     for core in range(tp_size):
-        middle = middle + jnp.dot(
-            mix_wide[core].astype(BF16), w_out_v[core], preferred_element_type=F32
+        mixed = jnp.concatenate([mix_wide[core, seq] for seq in range(seqs)], axis=0)
+        middle = middle + jnp.dot(mixed.astype(BF16), w_out_v[core], preferred_element_type=F32)
+    mid_src[...] = middle.astype(BF16)
+    for column in far_columns:
+        for device in cores(column):
+            remote(mid_src, mid_dst.at[me], 4, recv_wide.at[kv], device).start()
+    remote(mid_src, mid_dst.at[me], 4, recv_wide.at[kv], mate_device).start()
+
+    own_mid = mid_src[...].astype(F32)
+    mid_dst[pl.ds(me, 1)] = mid_src[...][None]
+    upward, squares = None, None
+    for column in [kv] + near_columns:
+        if upward is None:
+            arrived(mid_dst.at[kv * tp_size + mate], recv_wide.at[kv])
+        else:
+            arrived(mid_dst.at[duo(column)], recv_wide.at[column])
+        block = jnp.concatenate(
+            [mid_dst[column * tp_size + core].astype(F32) for core in range(tp_size)], axis=1
         )
-    mid_src[...] = middle.astype(BF16)
-    for other, device in far_peers:
-        send(mid_src, mid_dst.at[me], send_mid.at[other], recv_mid.at[me], device)
-
-    loads[10].wait()
-    loads[11].wait()
-    own_mid = mid_src[...].astype(F32)
-    squares = folded(own_mid)
-    upward = jnp.dot(
-        (own_mid * mixer_v[:, span(me)]).astype(BF16),
-        w_up_v[span(me), :],
-        preferred_element_type=F32,
-    )
-    for other, device in near_peers:
-        arrived(mid_src, mid_dst.at[other], send_mid.at[other], recv_mid.at[other], device)
-        block = mid_dst[other].astype(F32)
-        squares = squares + folded(block)
-        upward = upward + jnp.dot(
-            (block * mixer_v[:, span(other)]).astype(BF16),
-            w_up_v[span(other), :],
-            preferred_element_type=F32,
-        )
-    upward = upward * lax.rsqrt(jnp.sum(squares, axis=-1, keepdims=True) / width + 1e-06)
+        product = gained(block, mixer_v, w_up_v, column)
+        upward = product if upward is None else upward + product
+        squares = folded(block) if squares is None else squares + folded(block)
     activated = jnp.square(jnp.maximum(upward, 0.0)).astype(BF16)
-    loads[12].wait()
-
-    def down_piece(other):
-        return jnp.dot(activated, w_down_v[:, span(other)], preferred_element_type=F32)
-
-    for other, device in far_peers:
-        red_src[other] = down_piece(other).astype(BF16)
-        send(red_src.at[other], red_dst.at[me], send_red.at[other], recv_red.at[me], device)
-    done = own_mid + down_piece(me)
-    for other, device in near_peers:
-        arrived(red_src.at[other], red_dst.at[other], send_red.at[other], recv_red.at[other], device)
-        done = done + red_dst[other].astype(F32)
+    inverse = lax.rsqrt(jnp.sum(squares, axis=-1, keepdims=True) / width + 1e-06)
+    inverse = inverse * inverse
+
+    def down_halves(column):
+        both = jnp.dot(activated, w_down_v[:, span(column)], preferred_element_type=F32) * inverse
+        return [both[:, core * piece : (core + 1) * piece] for core in range(tp_size)]
+
+    for column in far_columns:
+        halves = down_halves(column)
+        for core, device in enumerate(cores(column)):
+            spot = column * tp_size + core
+            red_src[spot] = halves[core].astype(BF16)
+            remote(red_src.at[spot], red_dst.at[me], 5, recv_near.at[kv], device).start()
+    halves = down_halves(kv)
+    for core in range(tp_size):
+        red_src[kv * tp_size + core] = halves[core].astype(BF16)
+    own_mate = kv * tp_size + mate
+    remote(red_src.at[own_mate], red_dst.at[me], 5, recv_near.at[kv], mate_device).start()
+    done = halves[0]
+    for core in range(1, tp_size):
+        done = jnp.where(tp == core, halves[core], done)
+    done = own_mid + done
+    for column in [kv] + near_columns:
+        if column is kv:
+            arrived(red_dst.at[own_mate], recv_near.at[kv])
+            done = done + red_dst[own_mate].astype(F32)
+        else:
+            arrived(red_dst.at[duo(column)], recv_near.at[column])
+            for core in range(tp_size):
+                done = done + red_dst[column * tp_size + core].astype(F32)
     slot_of = lax.broadcasted_iota(jnp.int32, (slots, piece), 0)
     for seq in range(seqs):
         kept_rows = jnp.where(
             slot_of < lengths_s[seq], done[seq * slots : (seq + 1) * slots], 0.0
         )
         result[seq] = kept_rows.astype(BF16)
-    for copy in sent:
-        copy.wait_send()
+    others = pl.ds(0, group - 1)
+    for phase, ref in (
+        (0, tok_all.at[others]),
+        (1, w_out_v.at[0]),
+        (2, swap_dst.at[pl.ds(0, kv_size - 1)]),
+        (3, mix_dst.at[others]),
+        (4, mid_dst.at[others]),
+        (5, red_dst.at[others]),
+    ):
+        remote(ref, ref, phase, recv_out.at[0], mate_device).wait_send()
 
 
 def store_kernel(result, new_state, result_out, state_out, store_sem):
@@ -502,30 +554,25 @@
             vmem((model, hidden), BF16),
             vmem((hidden, model), BF16),
             vmem((seqs, 4 * slots, cols), F32),
+            vmem((seqs, slots, chans), F32),
             vmem((seqs, 4 * slots, cols), BF16),
             vmem((kv_size, 4 * slots, cols), BF16),
             vmem((4 * slots, heads, chans), F32),
             vmem((slots, heads, chans), F32),
             vmem((slots, heads * chans), BF16),
             vmem((group, slots, heads * chans), BF16),
-            vmem((tp_size, rows, heads * chans), F32),
+            vmem((tp_size, kv_size, slots, heads * chans), F32),
             vmem((rows, piece), BF16),
             vmem((group, rows, piece), BF16),
             vmem((group, rows, piece), BF16),
             vmem((group, rows, piece), BF16),
-            dma((14,)),
-            dma((group,)),
-            dma((group,)),
+            dma((9,)),
+            pltpu.SemaphoreType.REGULAR((kv_size,)),
+            dma((6,)),
             dma((1,)),
             dma((1,)),
             dma((kv_size,)),
             dma((kv_size,)),
-            dma((group,)),
-            dma((group,)),
-            dma((group,)),
-            dma((group,)),
-            dma((group,)),
-            dma((group,)),
         ],
         compiler_params=pltpu.CompilerParams(
             collective_id=0, has_side_effects=True, vmem_limit_bytes=56000 * 1024

time: 27.4 us -> 27.5 us (level)
  no operation moved by 1% of the time
where the time goes in v2:
time: 27.5 us; the launch traced here: 27.3 us
  Pallas kernels  26.6 us (97%)
  between operations  0.64 us (2%)
    pallas_call x1, Pallas kernels, local_kernel(): pl.pallas_call(functools.partial(step_kernel, kv_size, tp_size), out_shap...  25.8 us
    pallas_call x1, Pallas kernels, local_kernel(): pl.pallas_call(store_kernel, out_shape=(jax.ShapeDtypeStruct(tokens.shape...  0.83 us

profile of v2, /device:TPU:0, one launch (start us, length us, event | category | flops | bytes accessed | tf_op | source)
XLA Modules:
  0.0 27.3 jit_solution(11230031565767139202)
XLA Ops:
  0.6 25.8 %shard_map.149 = (bf16[4,4,256]{2,1,0:T(4,128)(2,1)S(1)}, f32[8,128,128]{2,1,0:T(8,128)S(1)}) custom-call(bf16[4,4,256]{2,1,0:T(4,128)(2,1)} %tokens.1, s32[4]{0:T(128)} %lengths.1, f32[8,128,128]{2,1,0:T(8,128)} %bitcast.23, f32[1,2048]{1,0:T(1,128)} %bitcast.24, bf16[256,2048]{1,0:T(8,128)(2,1)} %bitcast.18, bf16[256,2048]{1,0:T(8,128)(2,1)} %bitcast.19, ...), custom_call_target="tpu_custom_call" | custom-call | tf_op jit(solution)/shard_map/pallas_call | solution.py:534
  26.4 0.8 %shard_map.150 = (bf16[4,4,256]{2,1,0:T(4,128)(2,1)}, f32[8,128,128]{2,1,0:T(8,128)}) custom-call(bf16[4,4,256]{2,1,0:T(4,128)(2,1)S(1)} %get-tuple-element.6.result, f32[8,128,128]{2,1,0:T(8,128)S(1)} %get-tuple-element.7.new_state), custom_call_target="tpu_custom_call" | custom-call | tf_op jit(solution)/shard_map/pallas_call | solution.py:596
